TPU v7x, 32 devices: a whole 2x2x4 slice. The times are simulated.
32 devices in a mesh: ep: 32 (over z, y, x, core).
Axes of the slice: x: 2, y: 2, z: 4, core: 2. Of those that a mesh axis runs over, the one named last changes fastest.
Arguments:
- tokens: bfloat16 [256, 2048], P('ep'), may hold values from -6 to 6
- norm_gain: float32 [2048], replicated, may hold values from 0.1 to 1.9
- expert_gate: bfloat16 [32, 2048, 640], P('ep'), may hold values from -0.125 to 0.125
- expert_up: bfloat16 [32, 2048, 640], P('ep'), may hold values from -0.125 to 0.125
- expert_down: bfloat16 [32, 640, 2048], P('ep'), may hold values from -0.25 to 0.25
- shared_gate: bfloat16 [2048, 512], P(None, 'ep'), may hold values from -0.125 to 0.125
- shared_up: bfloat16 [2048, 512], P(None, 'ep'), may hold values from -0.125 to 0.125
- shared_down: bfloat16 [512, 2048], P('ep'), may hold values from -0.25 to 0.25
- branch_gate: bfloat16 [2048], replicated, may hold values from -0.125 to 0.125
- route_expert: int32 [256, 8], P('ep'), may hold values from 0 to 31, all different within a row; in each aligned block of 8 rows (0 to 7, 8 to 15, ...) at most 2 rows name the same one
- route_weight: float32 [256, 8], P('ep'), may hold values from 0.05 to 0.5
Outputs:
- mixed: bfloat16 [256, 2048], P('ep')
Inputs may be any that keep to these rules, and one draw needn't show every extreme that they name: `route_expert`: each row names 8 different experts; the rows of one device name one expert at most 2 times.
All inputs are finite; a program needn't handle non-finite values.
Results may differ from a plain program's by a relative error of at most 0.0085.
Values may be sent and summed in bfloat16 or wider, within the bound.
A program may use at most 128 MiB of HBM per device.

v0:
```python
import jax
import jax.numpy as jnp
from jax import lax
from jax.sharding import PartitionSpec as P


def norm_rows(tokens, norm_gain):
    values = tokens.astype(jnp.float32)
    scale = lax.rsqrt(jnp.mean(values * values, axis=-1, keepdims=True) + 1e-06)
    return (values * scale * norm_gain).astype(jnp.bfloat16)


def swiglu(rows, w_gate, w_up):
    return (
        jax.nn.silu(jnp.dot(rows, w_gate, preferred_element_type=jnp.float32))
        * jnp.dot(rows, w_up, preferred_element_type=jnp.float32)
    ).astype(jnp.bfloat16)


def per_device(
    tokens,
    norm_gain,
    expert_gate,
    expert_up,
    expert_down,
    shared_gate,
    shared_up,
    shared_down,
    branch_gate,
    route_expert,
    route_weight,
):
    tok_rows = tokens.shape[0]
    width = tokens.shape[1]
    topk = route_expert.shape[1]
    devices = lax.axis_size("ep")
    cap = max(1, (tok_rows * topk + devices - 1) // devices)
    limit = devices * cap
    normed = norm_rows(tokens, norm_gain)
    gate_all, up_all, down_all = (
        lax.all_gather(shared_gate, "ep", axis=1, tiled=True),
        lax.all_gather(shared_up, "ep", axis=1, tiled=True),
        lax.all_gather(shared_down, "ep", axis=0, tiled=True),
    )
    flat = route_expert.reshape(-1)
    hits = (flat[:, None] == jnp.arange(devices, dtype=jnp.int32)[None, :]).astype(jnp.int32)
    rank = jnp.sum((jnp.cumsum(hits, axis=0) - 1) * hits, axis=1)
    target = (flat * cap + rank).reshape(tok_rows, topk)
    slots = jnp.arange(limit, dtype=jnp.int32)
    select = jnp.any(target[None, :, :] == slots[:, None, None], axis=2).astype(jnp.bfloat16)
    sending = (
        jnp.dot(select, normed, preferred_element_type=jnp.float32)
        .astype(jnp.bfloat16)
        .reshape(devices, cap, width)
    )
    received = lax.all_to_all(sending, "ep", split_axis=0, concat_axis=0, tiled=True)
    hidden = swiglu(received.reshape(-1, width), expert_gate[0], expert_up[0])
    output = (
        jnp.dot(hidden, expert_down[0], preferred_element_type=jnp.float32)
        .astype(jnp.bfloat16)
        .reshape(received.shape)
    )
    returned = lax.all_to_all(output, "ep", split_axis=0, concat_axis=0, tiled=True).reshape(
        limit, width
    )
    picked = returned[target]
    moe_local = jnp.einsum("tk,tkd->td", route_weight, picked.astype(jnp.float32))
    own_hidden = swiglu(normed, gate_all, up_all)
    own_gate = jax.nn.sigmoid(jnp.dot(normed, branch_gate, preferred_element_type=jnp.float32))
    dense_own = own_gate[:, None] * jnp.dot(
        own_hidden, down_all, preferred_element_type=jnp.float32
    )
    return (moe_local + dense_own).astype(jnp.bfloat16)


def solution(mesh):
    placed = (
        P("ep", None),
        P(),
        P("ep", None, None),
        P("ep", None, None),
        P("ep", None, None),
        P(None, "ep"),
        P(None, "ep"),
        P("ep", None),
        P(),
        P("ep", None),
        P("ep", None),
    )
    return jax.shard_map(
        per_device, mesh=mesh, in_specs=placed, out_specs=P("ep", None), check_vma=False
    )
```

profile of v0, /device:TPU:0, one launch (start us, length us, event | category | flops | bytes accessed | tf_op | source)
XLA Modules:
  0.0 196.6 jit_solution(14969107579865949005)
XLA Ops:
  6.5 0.0 copy-start
  6.5 0.0 all-gather.4.cloned.1.call-start
  6.5 0.7 all-gather.4.cloned.1.call-update
  7.3 0.0 all-gather.6.cloned.1.call-start
  7.3 0.7 all-gather.6.cloned.1.call-update
  8.0 0.0 all-gather.8.cloned.1.call-start
  8.1 0.7 all-gather.8.cloned.1.call-update
  8.7 0.8 eq.28
  9.5 0.1 fusion.35
  9.6 0.1 reduce_window_sum.11
  9.7 0.2 select_reduce_fusion
  9.9 0.1 reduce_sum.21
  9.9 0.7 compare_select_fusion
  10.7 0.1 fusion.36
  10.7 0.9 fusion.32
  11.6 1.0 convolution_convert_fusion
  12.7 0.2 reshape.32
  12.9 18.8 %all_to_all.10 = bf16[32,2,2048]{2,1,0:T(2,128)(2,1)S(1)} all-to-all(bf16[32,2,2048]{2,1,0:T(2,128)(2,1)S(1)} %reshape.32), channel_id=1, replica_groups=mesh['ep'=32] {'ep'}, dimensions={0} | all-to-all | bytes 524288 | tf_op jit(solution)/shard_map/all_to_all | solution.py:56
  31.7 0.1 reshape.33
  31.8 2.3 %fusion.4 = f32[64,640]{1,0:T(8,128)S(1)} fusion(bf16[64,2048]{1,0:T(8,128)(2,1)S(1)} %reshape.33, bf16[1,2048,640]{2,1,0:T(8,128)(2,1)} %param.13), kind=kOutput, calls=%fused_computation.5 | convolution fusion | flops 167772160 | bytes 3047424 | tf_op jit(solution)/shard_map/dot_general | solution.py:15
  34.1 0.0 copy-done
  34.1 0.0 copy-start.3
  34.1 0.0 copy-start.1
  34.1 0.0 copy-start.2
  34.2 2.8 %fusion.6 = bf16[64,2048]{1,0:T(8,128)(2,1)S(1)} fusion(bf16[1,640,2048]{2,1,0:T(8,128)(2,1)S(1)} %copy-done, bf16[64,2048]{1,0:T(8,128)(2,1)S(1)} %reshape.33, bf16[1,2048,640]{2,1,0:T(8,128)(2,1)} %param.14, f32[64,640]{1,0:T(8,128)S(1)} %fusion.4), kind=kOutput, calls=%fused_computation.7 | convolution fusion | flops 335921152 | bytes 5931008 | tf_op jit(solution)/shard_map/dot_general | solution.py:59
  37.0 0.0 copy-start.4
  37.0 0.9 reshape.34
  37.8 2.6 %all-to-all-start.1 = ((bf16[32,2,2048]{2,1,0:T(2,128)(2,1)}), bf16[32,2,2048]{2,1,0:T(2,128)(2,1)S(1)}, u32[]{:S(2)}, u32[]{:S(2)}) async-start(bf16[32,2,2048]{2,1,0:T(2,128)(2,1)} %reshape.34), calls=%async_computation.1 | async-start | bytes 524288 | tf_op jit(solution)/shard_map/all_to_all | solution.py:63
  40.4 0.1 reshape.38
  40.5 0.0 copy-done.3
  40.5 0.0 copy-done.1
  40.5 0.0 copy-done.2
  40.6 0.2 fusion.21
  40.8 11.9 %all-to-all-done.1 = bf16[32,2,2048]{2,1,0:T(2,128)(2,1)S(1)} async-done(((bf16[32,2,2048]{2,1,0:T(2,128)(2,1)}), bf16[32,2,2048]{2,1,0:T(2,128)(2,1)S(1)}, u32[]{:S(2)}, u32[]{:S(2)}) %all-to-all-start.1) | async-done | bytes 262176 | tf_op jit(solution)/shard_map/all_to_all | solution.py:63
  52.7 0.1 reshape.35
  52.8 0.7 gather_fusion
  53.5 0.0 copy-done.4
  53.5 0.2 fusion.24
  53.8 16.6 %all-gather.4.cloned.1.call-done = bf16[2048,512]{0,1:T(8,128)(2,1)} async-done(((bf16[2048,16]{0,1:T(8,128)(2,1)}), bf16[2048,512]{0,1:T(8,128)(2,1)}) %all-gather.4.cloned.1.call-update) | async-done | bytes 2097168 | tf_op jit(solution)/shard_map/all_gather | solution.py:41
  70.3 2.2 %fusion.47 = f32[8,512]{1,0:T(8,128)S(1)} fusion(bf16[2048,512]{0,1:T(8,128)(2,1)} %all-gather.4.cloned.1.call-done, bf16[8,2048]{1,0:T(8,128)(2,1)S(1)} %copy-done.1, f32[2048]{0:T(1024)S(1)} %copy-done.2, f32[8]{0:T(128)S(1)} %add_rsqrt_fusion), kind=kOutput, calls=%fused_computation.51 | convolution fusion | flops 16842752 | bytes 2154528 | tf_op jit(solution)/shard_map/dot_general | solution.py:15
  72.5 55.7 %all-gather.6.cloned.1.call-done = bf16[2048,512]{0,1:T(8,128)(2,1)} async-done(((bf16[2048,16]{0,1:T(8,128)(2,1)}), bf16[2048,512]{0,1:T(8,128)(2,1)}) %all-gather.6.cloned.1.call-update) | async-done | bytes 2097168 | tf_op jit(solution)/shard_map/all_gather | solution.py:42
  128.3 57.9 %all-gather.8.cloned.1.call-done = bf16[512,2048]{1,0:T(8,128)(2,1)} async-done(((bf16[16,2048]{1,0:T(8,128)(2,1)}), bf16[512,2048]{1,0:T(8,128)(2,1)}) %all-gather.8.cloned.1.call-update) | async-done | bytes 2097168 | tf_op jit(solution)/shard_map/all_gather | solution.py:43
  186.2 3.8 %fusion.10 = bf16[8,2048]{1,0:T(8,128)(2,1)} fusion(bf16[512,2048]{1,0:T(8,128)(2,1)} %all-gather.8.cloned.1.call-done, bf16[2048,512]{0,1:T(8,128)(2,1)} %all-gather.6.cloned.1.call-done, f32[8,1,2048]{2,1,0:T(1,128)S(1)} %fusion.24, f32[8]{0:T(128)S(1)} %fusion.21, f32[8,512]{1,0:T(8,128)S(1)} %fusion.47, bf16[8,2048]{1,0:T(8,128)(2,1)S(1)} %copy-done.1, ...), kind=kOutput, calls=%fused_computation.11 | convolution fusion | flops 33693696 | bytes 4350016 | tf_op jit(solution)/shard_map/dot_general | solution.py:70
  (3 shorter events, 0.0 us)
Async XLA Ops:
  6.5 27.6 %copy-start = (bf16[1,640,2048]{2,1,0:T(8,128)(2,1)S(1)}, bf16[1,640,2048]{2,1,0:T(8,128)(2,1)}, u32[]{:S(2)}) copy-start(bf16[1,640,2048]{2,1,0:T(8,128)(2,1)} %param.15) | copy-start | bytes 7864324
  6.5 63.8 %all-gather.4.cloned.1.call-start = ((), (), s32[]{:S(2)}) async-start(), calls=%async_computation.2 | async-start | bytes 2162688 | tf_op jit(solution)/shard_map/all_gather | solution.py:41
  7.3 121.0 %all-gather.6.cloned.1.call-start = ((), (), s32[]{:S(2)}) async-start(), calls=%async_computation.3 | async-start | bytes 2162688 | tf_op jit(solution)/shard_map/all_gather | solution.py:42
  8.0 178.2 %all-gather.8.cloned.1.call-start = ((), (), s32[]{:S(2)}) async-start(), calls=%async_computation.4 | async-start | bytes 2162688 | tf_op jit(solution)/shard_map/all_gather | solution.py:43
  34.1 6.4 %copy-start.3 = (bf16[2048]{0:T(1024)(128)(2,1)S(1)}, bf16[2048]{0:T(1024)(128)(2,1)}, u32[]{:S(2)}) copy-start(bf16[2048]{0:T(1024)(128)(2,1)} %param.19) | copy-start | bytes 12292
  34.1 6.4 %copy-start.1 = (bf16[8,2048]{1,0:T(8,128)(2,1)S(1)}, bf16[8,2048]{1,0:T(8,128)(2,1)}, u32[]{:S(2)}) copy-start(bf16[8,2048]{1,0:T(8,128)(2,1)} %param.11) | copy-start | bytes 98308
  34.1 6.4 %copy-start.2 = (f32[2048]{0:T(1024)S(1)}, f32[2048]{0:T(1024)}, u32[]{:S(2)}) copy-start(f32[2048]{0:T(1024)} %param.12) | copy-start | bytes 24580
  37.0 16.6 %copy-start.4 = (f32[8,8]{1,0:T(8,128)S(1)}, f32[8,8]{1,0:T(8,128)}, u32[]{:S(2)}) copy-start(f32[8,8]{1,0:T(8,128)} %param.21) | copy-start | bytes 772
  37.8 14.8 %all-to-all-start.1 = ((bf16[32,2,2048]{2,1,0:T(2,128)(2,1)}), bf16[32,2,2048]{2,1,0:T(2,128)(2,1)S(1)}, u32[]{:S(2)}, u32[]{:S(2)}) async-start(bf16[32,2,2048]{2,1,0:T(2,128)(2,1)} %reshape.34), calls=%async_computation.1 | async-start | bytes 524288 | tf_op jit(solution)/shard_map/all_to_all | solution.py:63
Sparse Core Ops, SparseCore 0:
  10.2 60.0 all-gather.3
  73.2 55.0 all-gather.5
  131.1 55.0 all-gather.7
where the time goes:
time: 197 us
  waiting for transfers between devices  144 us (73%)
  blocking collectives  18.8 us (10%)
  between operations  13.2 us (7%)
  matrix products  12.6 us (6%)
  local copies, waits for them, and re-layouts  2.96 us (2%)
  starting transfers between devices  2.66 us (1%)
  other arithmetic  2.05 us (1%)
    all_gather x1, waiting for transfers between devices, per_device(): lax.all_gather(shared_down, 'ep', axis=0, tiled=True)  57.9 us
    all_gather x1, waiting for transfers between devices, per_device(): lax.all_gather(shared_up, 'ep', axis=1, tiled=True)  55.7 us
    all_to_all x1, blocking collectives, per_device(): lax.all_to_all(sending, 'ep', split_axis=0, concat_axis=0, tiled=True)  18.8 us
    all_gather x1, waiting for transfers between devices, per_device(): lax.all_gather(shared_gate, 'ep', axis=1, tiled=True)  16.6 us
    all_to_all x1, waiting for transfers between devices, per_device(): lax.all_to_all(output, 'ep', split_axis=0, concat_axis=0, tiled=True)  11.9 us
    dot_general x2, matrix products, swiglu(): jnp.dot(rows, w_gate, preferred_element_type=jnp.float32)  4.51 us
  transfers between devices with their start and end apart: 4, of which 4 were waited for; matrix products, arithmetic and copies ran while one was open for 7% of the time, Pallas kernels for 0%

commit v1 on v0

v1 whole, which is shorter than its diff:
```python
import functools

import jax
import jax.numpy as jnp
from jax import lax
from jax.experimental import pallas as pl
from jax.experimental.pallas import tpu as pltpu
from jax.sharding import PartitionSpec as P

F32 = jnp.float32
BF16 = jnp.bfloat16


def silu_pair(gate, up):
    return (gate / (1.0 + jnp.exp(-gate)) * up).astype(BF16)


def kernel(
    n,
    tokens,
    gain,
    branch,
    route,
    weight,
    e_gate,
    e_up,
    e_down,
    s_gate,
    s_up,
    s_down,
    out,
    toks,
    side,
    wg,
    wu,
    wd,
    sgu,
    sd,
    mine,
    theirs,
    given,
    sending,
    landed,
    w_sem,
    ts,
    tr,
    ss,
    sr,
    fts,
    ftr,
    fss,
    fsr,
    ps,
    pr,
    rs,
    rr,
):
    half = n // 2
    me = lax.axis_index("ep")
    core = lax.rem(me, 2)
    chip = me // 2
    partner = me + 1 - 2 * core

    loads = [
        pltpu.make_async_copy(src, dst, w_sem.at[i])
        for i, (src, dst) in enumerate(
            (
                (e_gate.at[0], wg),
                (e_up.at[0], wu),
                (s_gate, sgu.at[0]),
                (s_up, sgu.at[1]),
                (s_down, sd),
                (e_down.at[0], wd),
            )
        )
    ]
    for load in loads:
        load.start()

    def device_at(d):
        return lax.rem(chip + d, half) * 2 + core

    barrier = pltpu.get_barrier_semaphore()

    @pl.loop(1, half)
    def _(d):
        pl.semaphore_signal(barrier, inc=1, device_id={"ep": device_at(d)})

    pl.semaphore_signal(barrier, inc=1, device_id={"ep": partner})

    values = tokens[...].astype(F32)
    scale = lax.rsqrt(jnp.mean(values * values, axis=-1, keepdims=True) + 1e-06)
    normed = (values * scale * gain[...]).astype(BF16)
    toks[0, 0] = normed
    score = jnp.sum(normed.astype(F32) * branch[...].astype(F32).reshape(1, -1), axis=-1, keepdims=True)
    lane = lax.broadcasted_iota(jnp.int32, side.shape[2:], 1)
    table = jnp.where(lane == n, 1.0 / (1.0 + jnp.exp(-score)), 0.0)
    for k in range(route.shape[1]):
        table += jnp.where(lane == route[:, k : k + 1], weight[:, k : k + 1], 0.0)
    side[0, 0] = table

    pl.semaphore_wait(barrier, half)

    def spread(d):
        to = {"ep": device_at(d)}
        return (
            pltpu.make_async_remote_copy(
                toks.at[0, 0], toks.at[0, d], ts.at[d], tr.at[d], device_id=to
            ),
            pltpu.make_async_remote_copy(
                side.at[0, 0], side.at[0, d], ss.at[d], sr.at[d], device_id=to
            ),
        )

    def forward(d):
        to = {"ep": partner}
        return (
            pltpu.make_async_remote_copy(
                toks.at[0, d], toks.at[1, d], fts.at[d], ftr.at[d], device_id=to
            ),
            pltpu.make_async_remote_copy(
                side.at[0, d], side.at[1, d], fss.at[d], fsr.at[d], device_id=to
            ),
        )

    @pl.loop(1, half)
    def _(d):
        for copy in spread(d):
            copy.start()

    for copy in forward(0):
        copy.start()

    @pl.loop(1, half)
    def _(d):
        for copy in spread(d):
            copy.wait_recv()
        for copy in forward(d):
            copy.start()

    for load in loads:
        load.wait()

    @pl.loop(0, half)
    def _(d):
        for copy in forward(d):
            copy.wait_recv()

    def combined(which):
        rows = half * toks.shape[2]
        x = toks[which].reshape(rows, toks.shape[3])
        facts = side[which].reshape(rows, side.shape[3])
        spot = lax.broadcasted_iota(jnp.int32, facts.shape, 1)
        share = jnp.sum(jnp.where(spot == me, facts, 0.0), axis=1, keepdims=True)
        gate = jnp.sum(jnp.where(spot == n, facts, 0.0), axis=1, keepdims=True)
        dot = functools.partial(jnp.dot, preferred_element_type=F32)
        hidden = silu_pair(dot(x, wg[...]), dot(x, wu[...]))
        units = sgu.shape[1]
        pair = lax.dot_general(
            x,
            sgu[...].reshape(2 * units, sgu.shape[2]),
            (((1,), (1,)), ((), ())),
            preferred_element_type=F32,
        )
        dense_hidden = silu_pair(pair[:, :units], pair[:, units:])
        routed = dot(hidden, wd[...]).astype(BF16).astype(F32)
        return share * routed + gate * dot(dense_hidden, sd[...])

    theirs[...] = combined(1).astype(BF16).reshape(theirs.shape)
    swap = pltpu.make_async_remote_copy(
        theirs, given, ps, pr, device_id={"ep": partner}
    )
    swap.start()
    mine[...] = combined(0).reshape(mine.shape)
    swap.wait_recv()
    total = mine[...] + given[...].astype(F32)
    sending[...] = total.astype(BF16)

    def home(d):
        return pltpu.make_async_remote_copy(
            sending.at[d],
            landed.at[d],
            rs.at[d],
            rr.at[d],
            device_id={"ep": lax.rem(chip - d + half, half) * 2 + core},
        )

    @pl.loop(1, half)
    def _(d):
        home(d).start()

    mine[0] = total[0]

    @pl.loop(1, half)
    def _(d):
        for copy in spread(d):
            copy.wait_send()

    @pl.loop(0, half)
    def _(d):
        for copy in forward(d):
            copy.wait_send()

    swap.wait_send()

    @pl.loop(1, half)
    def _(d):
        home(d).wait_recv()
        mine[0] += landed[d].astype(F32)

    out[...] = mine[0].astype(BF16)

    @pl.loop(1, half)
    def _(d):
        home(d).wait_send()


def per_device(
    tokens,
    norm_gain,
    expert_gate,
    expert_up,
    expert_down,
    shared_gate,
    shared_up,
    shared_down,
    branch_gate,
    route_expert,
    route_weight,
):
    n = lax.axis_size("ep")
    half = n // 2
    rows, width = tokens.shape
    lanes = (n + 1 + 127) // 128 * 128
    vmem = pl.BlockSpec(memory_space=pltpu.VMEM)
    anywhere = pl.BlockSpec(memory_space=pl.ANY)
    dma = pltpu.SemaphoreType.DMA
    return pl.pallas_call(
        functools.partial(kernel, n),
        out_shape=jax.ShapeDtypeStruct((rows, width), BF16),
        in_specs=[vmem] * 5 + [anywhere] * 6,
        out_specs=vmem,
        scratch_shapes=[
            pltpu.VMEM((2, half, rows, width), BF16),
            pltpu.VMEM((2, half, rows, lanes), F32),
            pltpu.VMEM(expert_gate.shape[1:], BF16),
            pltpu.VMEM(expert_up.shape[1:], BF16),
            pltpu.VMEM(expert_down.shape[1:], BF16),
            pltpu.VMEM((2,) + shared_gate.shape[::-1], BF16),
            pltpu.VMEM(shared_down.shape, BF16),
            pltpu.VMEM((half, rows, width), F32),
            pltpu.VMEM((half, rows, width), BF16),
            pltpu.VMEM((half, rows, width), BF16),
            pltpu.VMEM((half, rows, width), BF16),
            pltpu.VMEM((half, rows, width), BF16),
            dma((6,)),
        ]
        + [dma((half,))] * 8
        + [dma, dma]
        + [dma((half,))] * 2,
        compiler_params=pltpu.CompilerParams(
            collective_id=0, has_side_effects=True, vmem_limit_bytes=60 * 1024 * 1024
        ),
    )(
        tokens,
        norm_gain.reshape(1, -1),
        branch_gate,
        route_expert,
        route_weight,
        expert_gate,
        expert_up,
        expert_down,
        shared_gate.T,
        shared_up.T,
        shared_down,
    )


def solution(mesh):
    placed = (
        P("ep", None),
        P(),
        P("ep", None, None),
        P("ep", None, None),
        P("ep", None, None),
        P(None, "ep"),
        P(None, "ep"),
        P("ep", None),
        P(),
        P("ep", None),
        P("ep", None),
    )
    return jax.shard_map(
        per_device, mesh=mesh, in_specs=placed, out_specs=P("ep", None), check_vma=False
    )
```

time: 197 us -> 43.8 us (0.22)
  waiting for transfers between devices: 144 us -> 0 us
  Pallas kernels: 0 us -> 42.1 us
  blocking collectives: 18.8 us -> 0 us
  between operations: 13.2 us -> 0.01 us
  matrix products: 12.6 us -> 0 us
  starting transfers between devices: 2.66 us -> 0 us
  other arithmetic: 2.05 us -> 0 us
    all_gather x3 -> x0, waiting for transfers between devices: 130 us -> none  [the longest x1 57.9 us: per_device(): lax.all_gather(shared_down, 'ep', axis=0, tiled=True)]
    pallas_call x0 -> x1, Pallas kernels: none -> 42.1 us  [per_device(): pl.pallas_call(functools.partial(kernel, n), out_shape=jax.ShapeDtypeStru...]
    all_to_all x1 -> x0, blocking collectives: 18.8 us -> none  [per_device(): lax.all_to_all(sending, 'ep', split_axis=0, concat_axis=0, tiled=True)]
    dot_general x7 -> x0, matrix products: 12.6 us -> none  [the longest x2 4.51 us: swiglu(): jnp.dot(rows, w_gate, preferred_element_type=jnp.float32)]
    all_to_all x1 -> x0, waiting for transfers between devices: 11.9 us -> none  [per_device(): lax.all_to_all(output, 'ep', split_axis=0, concat_axis=0, tiled=True)]
    all_to_all x1 -> x0, starting transfers between devices: 2.58 us -> none  [per_device(): lax.all_to_all(output, 'ep', split_axis=0, concat_axis=0, tiled=True)]
    unnamed x3 -> x0, waiting for transfers between devices: 2.09 us -> none
  transfers between devices with their start and end apart: 4 -> 0, of which waited for: 4 -> 0; matrix products, arithmetic and copies ran while one was open for 7% -> 0% of each run, Pallas kernels for 0% -> 0%
where the time goes in v1:
time: 43.8 us; the launch traced here: 43.5 us
  Pallas kernels  42.1 us (96%)
  local copies, waits for them, and re-layouts  1.38 us (3%)
    pallas_call x1, Pallas kernels, per_device(): pl.pallas_call(functools.partial(kernel, n), out_shape=jax.ShapeDtypeStru...  42.1 us
    unnamed x1, local copies, waits for them, and re-layouts  1.38 us

profile of v1, /device:TPU:0, one launch (start us, length us, event | category | flops | bytes accessed | tf_op | source)
XLA Modules:
  0.0 43.5 jit_solution(14747185657944166891)
XLA Ops:
  0.0 42.1 %shard_map.109 = bf16[8,2048]{1,0:T(8,128)(2,1)} custom-call(bf16[8,2048]{1,0:T(8,128)(2,1)} %tokens.1, f32[1,2048]{1,0:T(1,128)} %bitcast.5, bf16[2048]{0:T(1024)(128)(2,1)} %branch.1, s32[8,8]{1,0:T(8,128)} %route.1, f32[8,8]{1,0:T(8,128)} %weight.1, bf16[1,2048,640]{2,1,0:T(8,128)(2,1)} %e_gate.1, bf16[1,2048,640]{2,1,0:T(8,128)(2,1)} %e_up.1, ...), custom_call_target="tpu_custom_call" | custom-call | tf_op jit(solution)/shard_map/pallas_call | solution.py:238
  42.2 1.4 %copy.13 = bf16[8,2048]{1,0:T(8,128)(2,1)} copy(bf16[8,2048]{1,0:T(8,128)(2,1)} %shard_map.109) | data formatting | bytes 65536

commit v2 on v1

v2 whole, which is shorter than its diff:
```python
import functools
import math

import jax
import jax.numpy as jnp
from jax import lax
from jax.experimental import pallas as pl
from jax.experimental.pallas import tpu as pltpu
from jax.sharding import PartitionSpec as P

F32 = jnp.float32
BF16 = jnp.bfloat16


def silu_pair(gate, up):
    return (gate / (1.0 + jnp.exp(-gate)) * up).astype(BF16)


def kernel(
    n,
    plane,
    tokens,
    gain,
    branch,
    route,
    weight,
    e_gate,
    e_up,
    e_down,
    s_gate,
    s_up,
    s_down,
    out,
    toks,
    wg,
    wu,
    wd,
    sgu,
    sd,
    mine,
    theirs,
    given,
    sending,
    landed,
    summed,
    arrived,
    w_sem,
    far_s,
    far_r,
    near_s,
    near_r,
    pass_s,
    pass_r,
    swap_s,
    swap_r,
    part_s,
    part_r,
    last_s,
    last_r,
):
    half = n // 2
    planes = half // plane
    width = tokens.shape[1]
    me = lax.axis_index("ep")
    core = lax.rem(me, 2)
    chip = me // 2
    low = lax.rem(chip, plane)
    high = chip // plane
    partner = {"ep": me + 1 - 2 * core}

    def at(a, b):
        row = lax.rem(high + a + planes, planes)
        column = lax.rem(low + b + plane, plane)
        return {"ep": (row * plane + column) * 2 + core}

    loads = [
        pltpu.make_async_copy(src, dst, w_sem.at[i])
        for i, (src, dst) in enumerate(
            (
                (e_gate.at[0], wg),
                (e_up.at[0], wu),
                (s_gate, sgu.at[0]),
                (s_up, sgu.at[1]),
                (s_down, sd),
                (e_down.at[0], wd),
            )
        )
    ]
    for load in loads:
        load.start()

    barrier = pltpu.get_barrier_semaphore()
    for a in range(1, planes):
        pl.semaphore_signal(barrier, inc=1, device_id=at(a, 0))
    for b in range(1, plane):
        pl.semaphore_signal(barrier, inc=1, device_id=at(0, b))
    pl.semaphore_signal(barrier, inc=1, device_id=partner)

    values = tokens[...].astype(F32)
    scale = lax.rsqrt(jnp.mean(values * values, axis=-1, keepdims=True) + 1e-06)
    normed = (values * scale * gain[...]).astype(BF16)
    score = jnp.sum(
        normed.astype(F32) * branch[...].astype(F32).reshape(1, -1), axis=-1, keepdims=True
    )

    def columns(shape):
        lane = lax.broadcasted_iota(jnp.int32, shape, 1)
        piece = (lane >= n + 1).astype(jnp.int32) + (lane >= 2 * (n + 1)).astype(jnp.int32)
        return piece, lane - piece * (n + 1)

    piece, column = columns((tokens.shape[0], toks.shape[4] - width))
    table = jnp.where(column == n, 1.0 / (1.0 + jnp.exp(-score)), 0.0)
    for k in range(route.shape[1]):
        table += jnp.where(column == route[:, k : k + 1], weight[:, k : k + 1], 0.0)
    first = table.astype(BF16).astype(F32)
    second = (table - first).astype(BF16).astype(F32)
    third = table - first - second
    pieces = jnp.where(piece == 0, first, jnp.where(piece == 1, second, third))
    toks[0, 0, 0, :, :width] = normed
    toks[0, 0, 0, :, width:] = pieces.astype(BF16)

    pl.semaphore_wait(barrier, planes + plane - 1)

    def far(a):
        return pltpu.make_async_remote_copy(
            toks.at[0, 0, 0],
            toks.at[0, 0, a],
            far_s.at[a],
            far_r.at[a],
            device_id=at(-a, 0),
        )

    def near(a, b):
        return pltpu.make_async_remote_copy(
            toks.at[0, 0, a],
            toks.at[0, b, a],
            near_s.at[b, a],
            near_r.at[b, a],
            device_id=at(0, -b),
        )

    def hand(a, b):
        return pltpu.make_async_remote_copy(
            toks.at[0, b, a],
            toks.at[1, b, a],
            pass_s.at[b, a],
            pass_r.at[b, a],
            device_id=partner,
        )

    order = sorted(range(1, planes), key=lambda a: min(a, planes - a))
    for a in order:
        far(a).start()
    for b in range(1, plane):
        near(0, b).start()
    hand(0, 0).start()
    for a in order:
        far(a).wait_recv()
        for b in range(1, plane):
            near(a, b).start()
        hand(a, 0).start()
    for a in [0] + order:
        for b in range(1, plane):
            near(a, b).wait_recv()
            hand(a, b).start()

    for load in loads:
        load.wait()

    for a in range(planes):
        for b in range(plane):
            hand(a, b).wait_recv()

    def combined(which):
        rows = half * tokens.shape[0]
        x = toks[which, :, :, :, :width].reshape(rows, width)
        facts = toks[which, :, :, :, width:].astype(F32).reshape(rows, -1)
        _, spot = columns(facts.shape)
        share = jnp.sum(jnp.where(spot == me, facts, 0.0), axis=1, keepdims=True)
        gate = jnp.sum(jnp.where(spot == n, facts, 0.0), axis=1, keepdims=True)
        dot = functools.partial(jnp.dot, preferred_element_type=F32)
        hidden = silu_pair(dot(x, wg[...]), dot(x, wu[...]))
        units = sgu.shape[1]
        pair = lax.dot_general(
            x,
            sgu[...].reshape(2 * units, width),
            (((1,), (1,)), ((), ())),
            preferred_element_type=F32,
        )
        dense_hidden = silu_pair(pair[:, :units], pair[:, units:])
        routed = dot(hidden, wd[...]).astype(BF16).astype(F32)
        return share * routed + gate * dot(dense_hidden, sd[...])

    theirs[...] = combined(1).astype(BF16).reshape(theirs.shape)
    swap = pltpu.make_async_remote_copy(theirs, given, swap_s, swap_r, device_id=partner)
    swap.start()
    mine[...] = combined(0).reshape(mine.shape)
    swap.wait_recv()
    for b in range(1, plane):
        sending[b] = (mine[b] + given[b].astype(F32)).astype(BF16)

    def part(a, b):
        return pltpu.make_async_remote_copy(
            sending.at[b, a],
            landed.at[b, a],
            part_s.at[b, a],
            part_r.at[b, a],
            device_id=at(0, b),
        )

    def last(a):
        return pltpu.make_async_remote_copy(
            summed.at[a], arrived.at[a], last_s.at[a], last_r.at[a], device_id=at(a, 0)
        )

    back = order[::-1]
    for a in back + [0]:
        for b in range(1, plane):
            part(a, b).start()

    def whole(a):
        total = mine[0, a] + given[0, a].astype(F32)
        for b in range(1, plane):
            part(a, b).wait_recv()
            total += landed[b, a].astype(F32)
        return total

    for a in back:
        summed[a] = whole(a).astype(BF16)
        last(a).start()
    result = whole(0)

    for a in order:
        far(a).wait_send()
    for a in range(planes):
        for b in range(plane):
            hand(a, b).wait_send()
            if b > 0:
                near(a, b).wait_send()
                part(a, b).wait_send()
    swap.wait_send()

    for a in back:
        last(a).wait_recv()
        result += arrived[a].astype(F32)
    out[...] = result.astype(BF16)
    for a in back:
        last(a).wait_send()


def per_device(
    tokens,
    norm_gain,
    expert_gate,
    expert_up,
    expert_down,
    shared_gate,
    shared_up,
    shared_down,
    branch_gate,
    route_expert,
    route_weight,
):
    n = lax.axis_size("ep")
    half = n // 2
    plane = math.isqrt(half)
    while half % plane:
        plane -= 1
    planes = half // plane
    rows, width = tokens.shape
    lanes = (3 * (n + 1) + 127) // 128 * 128
    vmem = pl.BlockSpec(memory_space=pltpu.VMEM)
    anywhere = pl.BlockSpec(memory_space=pl.ANY)
    dma = pltpu.SemaphoreType.DMA
    blocks = pltpu.VMEM((plane, planes, rows, width), BF16)
    return pl.pallas_call(
        functools.partial(kernel, n, plane),
        out_shape=jax.ShapeDtypeStruct((rows, width), BF16),
        in_specs=[vmem] * 5 + [anywhere] * 6,
        out_specs=vmem,
        scratch_shapes=[
            pltpu.VMEM((2, plane, planes, rows, width + lanes), BF16),
            pltpu.VMEM(expert_gate.shape[1:], BF16),
            pltpu.VMEM(expert_up.shape[1:], BF16),
            pltpu.VMEM(expert_down.shape[1:], BF16),
            pltpu.VMEM((2,) + shared_gate.shape[::-1], BF16),
            pltpu.VMEM(shared_down.shape, BF16),
            pltpu.VMEM((plane, planes, rows, width), F32),
            blocks,
            blocks,
            blocks,
            blocks,
            pltpu.VMEM((planes, rows, width), BF16),
            pltpu.VMEM((planes, rows, width), BF16),
            dma((6,)),
            dma((planes,)),
            dma((planes,)),
            dma((plane, planes)),
            dma((plane, planes)),
            dma((plane, planes)),
            dma((plane, planes)),
            dma,
            dma,
            dma((plane, planes)),
            dma((plane, planes)),
            dma((planes,)),
            dma((planes,)),
        ],
        compiler_params=pltpu.CompilerParams(
            collective_id=0, has_side_effects=True, vmem_limit_bytes=60 * 1024 * 1024
        ),
    )(
        tokens,
        norm_gain.reshape(1, -1),
        branch_gate,
        route_expert,
        route_weight,
        expert_gate,
        expert_up,
        expert_down,
        shared_gate.T,
        shared_up.T,
        shared_down,
    )


def solution(mesh):
    placed = (
        P("ep", None),
        P(),
        P("ep", None, None),
        P("ep", None, None),
        P("ep", None, None),
        P(None, "ep"),
        P(None, "ep"),
        P("ep", None),
        P(),
        P("ep", None),
        P("ep", None),
    )
    return jax.shard_map(
        per_device, mesh=mesh, in_specs=placed, out_specs=P("ep", None), check_vma=False
    )
```

time: 43.8 us -> 34.1 us (0.78)
  Pallas kernels: 42.1 us -> 32.4 us
    pallas_call x1, Pallas kernels: 42.1 us -> 32.4 us  [per_device(): pl.pallas_call(functools.partial(kernel, n, plane), out_shape=jax.ShapeDt...]
where the time goes in v2:
time: 34.1 us; the launch traced here: 33.8 us
  Pallas kernels  32.4 us (95%)
  local copies, waits for them, and re-layouts  1.38 us (4%)
    pallas_call x1, Pallas kernels, per_device(): pl.pallas_call(functools.partial(kernel, n, plane), out_shape=jax.ShapeDt...  32.4 us
    unnamed x1, local copies, waits for them, and re-layouts  1.38 us

profile of v2, /device:TPU:0, one launch (start us, length us, event | category | flops | bytes accessed | tf_op | source)
XLA Modules:
  0.0 33.8 jit_solution(1565393638674082318)
XLA Ops:
  0.0 32.4 %shard_map.109 = bf16[8,2048]{1,0:T(8,128)(2,1)} custom-call(bf16[8,2048]{1,0:T(8,128)(2,1)} %tokens.1, f32[1,2048]{1,0:T(1,128)} %bitcast.5, bf16[2048]{0:T(1024)(128)(2,1)} %branch.1, s32[8,8]{1,0:T(8,128)} %route.1, f32[8,8]{1,0:T(8,128)} %weight.1, bf16[1,2048,640]{2,1,0:T(8,128)(2,1)} %e_gate.1, bf16[1,2048,640]{2,1,0:T(8,128)(2,1)} %e_up.1, ...), custom_call_target="tpu_custom_call" | custom-call | tf_op jit(solution)/shard_map/pallas_call | solution.py:276
  32.4 1.4 %copy.13 = bf16[8,2048]{1,0:T(8,128)(2,1)} copy(bf16[8,2048]{1,0:T(8,128)(2,1)} %shard_map.109) | data formatting | bytes 65536

commit v3 on v2

--- a/solution.py
+++ b/solution.py
@@ -121,60 +121,70 @@
 
     pl.semaphore_wait(barrier, planes + plane - 1)
 
-    def far(a):
+    slots = [0] + sorted(range(1, planes), key=lambda a: min(a, planes - a))
+    middle = max(1, planes // 2)
+    chunks = [c for c in ((0, middle), (middle, planes)) if c[0] < c[1]]
+    others = range(1, planes)
+    peers = range(1, plane)
+
+    def far(i):
         return pltpu.make_async_remote_copy(
             toks.at[0, 0, 0],
-            toks.at[0, 0, a],
-            far_s.at[a],
-            far_r.at[a],
-            device_id=at(-a, 0),
-        )
-
-    def near(a, b):
-        return pltpu.make_async_remote_copy(
-            toks.at[0, 0, a],
-            toks.at[0, b, a],
-            near_s.at[b, a],
-            near_r.at[b, a],
+            toks.at[i, 0, 0],
+            far_s.at[i],
+            far_r.at[i],
+            device_id=at(-slots[i], 0),
+        )
+
+    def near(i, b):
+        return pltpu.make_async_remote_copy(
+            toks.at[i, 0, 0],
+            toks.at[i, 0, b],
+            near_s.at[b, i],
+            near_r.at[b, i],
             device_id=at(0, -b),
         )
 
-    def hand(a, b):
-        return pltpu.make_async_remote_copy(
-            toks.at[0, b, a],
-            toks.at[1, b, a],
-            pass_s.at[b, a],
-            pass_r.at[b, a],
+    def hand(i, b):
+        return pltpu.make_async_remote_copy(
+            toks.at[i, 0, b],
+            toks.at[i, 1, b],
+            pass_s.at[b, i],
+            pass_r.at[b, i],
             device_id=partner,
         )
 
-    order = sorted(range(1, planes), key=lambda a: min(a, planes - a))
-    for a in order:
-        far(a).start()
-    for b in range(1, plane):
-        near(0, b).start()
-    hand(0, 0).start()
-    for a in order:
-        far(a).wait_recv()
-        for b in range(1, plane):
-            near(a, b).start()
-        hand(a, 0).start()
-    for a in [0] + order:
-        for b in range(1, plane):
-            near(a, b).wait_recv()
-            hand(a, b).start()
-
-    for load in loads:
-        load.wait()
-
-    for a in range(planes):
-        for b in range(plane):
-            hand(a, b).wait_recv()
-
-    def combined(which):
-        rows = half * tokens.shape[0]
-        x = toks[which, :, :, :, :width].reshape(rows, width)
-        facts = toks[which, :, :, :, width:].astype(F32).reshape(rows, -1)
+    def swap(c):
+        low_i, high_i = chunks[c]
+        span = pl.ds(low_i, high_i - low_i)
+        return pltpu.make_async_remote_copy(
+            theirs.at[span], given.at[span], swap_s.at[c], swap_r.at[c], device_id=partner
+        )
+
+    def part(i, b):
+        return pltpu.make_async_remote_copy(
+            sending.at[i, b],
+            landed.at[i, b],
+            part_s.at[b, i],
+            part_r.at[b, i],
+            device_id=at(0, b),
+        )
+
+    def last(i):
+        return pltpu.make_async_remote_copy(
+            summed.at[i],
+            arrived.at[i],
+            last_s.at[i],
+            last_r.at[i],
+            device_id=at(slots[i], 0),
+        )
+
+    def compute(c):
+        low_i, high_i = chunks[c]
+        count = high_i - low_i
+        rows = count * 2 * plane * tokens.shape[0]
+        x = toks[low_i:high_i, :, :, :, :width].reshape(rows, width)
+        facts = toks[low_i:high_i, :, :, :, width:].astype(F32).reshape(rows, -1)
         _, spot = columns(facts.shape)
         share = jnp.sum(jnp.where(spot == me, facts, 0.0), axis=1, keepdims=True)
         gate = jnp.sum(jnp.where(spot == n, facts, 0.0), axis=1, keepdims=True)
@@ -189,63 +199,89 @@
         )
         dense_hidden = silu_pair(pair[:, :units], pair[:, units:])
         routed = dot(hidden, wd[...]).astype(BF16).astype(F32)
-        return share * routed + gate * dot(dense_hidden, sd[...])
-
-    theirs[...] = combined(1).astype(BF16).reshape(theirs.shape)
-    swap = pltpu.make_async_remote_copy(theirs, given, swap_s, swap_r, device_id=partner)
-    swap.start()
-    mine[...] = combined(0).reshape(mine.shape)
-    swap.wait_recv()
-    for b in range(1, plane):
-        sending[b] = (mine[b] + given[b].astype(F32)).astype(BF16)
-
-    def part(a, b):
-        return pltpu.make_async_remote_copy(
-            sending.at[b, a],
-            landed.at[b, a],
-            part_s.at[b, a],
-            part_r.at[b, a],
-            device_id=at(0, b),
-        )
-
-    def last(a):
-        return pltpu.make_async_remote_copy(
-            summed.at[a], arrived.at[a], last_s.at[a], last_r.at[a], device_id=at(a, 0)
-        )
-
-    back = order[::-1]
-    for a in back + [0]:
-        for b in range(1, plane):
-            part(a, b).start()
-
-    def whole(a):
-        total = mine[0, a] + given[0, a].astype(F32)
-        for b in range(1, plane):
-            part(a, b).wait_recv()
-            total += landed[b, a].astype(F32)
+        both = share * routed + gate * dot(dense_hidden, sd[...])
+        both = both.reshape(count, 2, *mine.shape[1:])
+        theirs[low_i:high_i] = both[:, 1].astype(BF16)
+        mine[low_i:high_i] = both[:, 0]
+        swap(c).start()
+
+    def collect(c):
+        for i in range(*chunks[c]):
+            for b in peers:
+                near(i, b).wait_recv()
+                hand(i, b).start()
+
+    def ready(c):
+        for i in range(*chunks[c]):
+            for b in range(plane):
+                hand(i, b).wait_recv()
+
+    def depart(c):
+        low_i, high_i = chunks[c]
+        swap(c).wait_recv()
+        mine[low_i:high_i] += given[low_i:high_i].astype(F32)
+        for b in peers:
+            sending[low_i:high_i, b] = mine[low_i:high_i, b].astype(BF16)
+        for i in range(low_i, high_i):
+            for b in peers:
+                part(i, b).start()
+
+    def whole(i):
+        total = mine[i, 0]
+        for b in peers:
+            part(i, b).wait_recv()
+            total += landed[i, b].astype(F32)
         return total
 
-    for a in back:
-        summed[a] = whole(a).astype(BF16)
-        last(a).start()
+    for i in others:
+        far(i).start()
+    for b in peers:
+        near(0, b).start()
+    hand(0, 0).start()
+    for i in others:
+        far(i).wait_recv()
+        for b in peers:
+            near(i, b).start()
+        hand(i, 0).start()
+
+    collect(0)
+    for load in loads:
+        load.wait()
+    ready(0)
+    compute(0)
+    for c in range(1, len(chunks)):
+        collect(c)
+        depart(c - 1)
+        ready(c)
+        compute(c)
+        for i in range(*chunks[c - 1]):
+            if i > 0:
+                summed[i] = whole(i).astype(BF16)
+                last(i).start()
+    depart(len(chunks) - 1)
+    for i in range(*chunks[-1]):
+        if i > 0:
+            summed[i] = whole(i).astype(BF16)
+            last(i).start()
     result = whole(0)
 
-    for a in order:
-        far(a).wait_send()
-    for a in range(planes):
+    for i in range(planes):
         for b in range(plane):
-            hand(a, b).wait_send()
+            hand(i, b).wait_send()
             if b > 0:
-                near(a, b).wait_send()
-                part(a, b).wait_send()
-    swap.wait_send()
-
-    for a in back:
-        last(a).wait_recv()
-        result += arrived[a].astype(F32)
+                near(i, b).wait_send()
+                part(i, b).wait_send()
+        if i > 0:
+            far(i).wait_send()
+    for c in range(len(chunks)):
+        swap(c).wait_send()
+
+    for i in others:
+        last(i).wait_recv()
+        result += arrived[i].astype(F32)
     out[...] = result.astype(BF16)
-    for a in back:
-        last(a).wait_send()
+    for i in others:
+        last(i).wait_send()
 
 
 def per_device(
@@ -272,20 +308,20 @@
     vmem = pl.BlockSpec(memory_space=pltpu.VMEM)
     anywhere = pl.BlockSpec(memory_space=pl.ANY)
     dma = pltpu.SemaphoreType.DMA
-    blocks = pltpu.VMEM((plane, planes, rows, width), BF16)
+    blocks = pltpu.VMEM((planes, plane, rows, width), BF16)
     return pl.pallas_call(
         functools.partial(kernel, n, plane),
         out_shape=jax.ShapeDtypeStruct((rows, width), BF16),
         in_specs=[vmem] * 5 + [anywhere] * 6,
         out_specs=vmem,
         scratch_shapes=[
-            pltpu.VMEM((2, plane, planes, rows, width + lanes), BF16),
+            pltpu.VMEM((planes, 2, plane, rows, width + lanes), BF16),
             pltpu.VMEM(expert_gate.shape[1:], BF16),
             pltpu.VMEM(expert_up.shape[1:], BF16),
             pltpu.VMEM(expert_down.shape[1:], BF16),
             pltpu.VMEM((2,) + shared_gate.shape[::-1], BF16),
             pltpu.VMEM(shared_down.shape, BF16),
-            pltpu.VMEM((plane, planes, rows, width), F32),
+            pltpu.VMEM((planes, plane, rows, width), F32),
             blocks,
             blocks,
             blocks,
@@ -299,8 +335,8 @@
             dma((plane, planes)),
             dma((plane, planes)),
             dma((plane, planes)),
-            dma,
-            dma,
+            dma((2,)),
+            dma((2,)),
             dma((plane, planes)),
             dma((plane, planes)),
             dma((planes,)),

time: 34.1 us -> 32.3 us (0.947)
  Pallas kernels: 32.4 us -> 30.6 us
    pallas_call x1, Pallas kernels: 32.4 us -> 30.6 us  [per_device(): pl.pallas_call(functools.partial(kernel, n, plane), out_shape=jax.ShapeDt...]
where the time goes in v3:
time: 32.3 us; the launch traced here: 32 us
  Pallas kernels  30.6 us (95%)
  local copies, waits for them, and re-layouts  1.38 us (4%)
    pallas_call x1, Pallas kernels, per_device(): pl.pallas_call(functools.partial(kernel, n, plane), out_shape=jax.ShapeDt...  30.6 us
    unnamed x1, local copies, waits for them, and re-layouts  1.38 us

profile of v3, /device:TPU:0, one launch (start us, length us, event | category | flops | bytes accessed | tf_op | source)
XLA Modules:
  0.0 32.0 jit_solution(12722641463410595244)
XLA Ops:
  0.0 30.6 %shard_map.109 = bf16[8,2048]{1,0:T(8,128)(2,1)} custom-call(bf16[8,2048]{1,0:T(8,128)(2,1)} %tokens.1, f32[1,2048]{1,0:T(1,128)} %bitcast.5, bf16[2048]{0:T(1024)(128)(2,1)} %branch.1, s32[8,8]{1,0:T(8,128)} %route.1, f32[8,8]{1,0:T(8,128)} %weight.1, bf16[1,2048,640]{2,1,0:T(8,128)(2,1)} %e_gate.1, bf16[1,2048,640]{2,1,0:T(8,128)(2,1)} %e_up.1, ...), custom_call_target="tpu_custom_call" | custom-call | tf_op jit(solution)/shard_map/pallas_call | solution.py:312
  30.7 1.4 %copy.13 = bf16[8,2048]{1,0:T(8,128)(2,1)} copy(bf16[8,2048]{1,0:T(8,128)(2,1)} %shard_map.109) | data formatting | bytes 65536

commit v4 on v3

--- a/solution.py
+++ b/solution.py
@@ -219,15 +219,15 @@
     def depart(c):
         low_i, high_i = chunks[c]
         swap(c).wait_recv()
-        mine[low_i:high_i] += given[low_i:high_i].astype(F32)
-        for b in peers:
-            sending[low_i:high_i, b] = mine[low_i:high_i, b].astype(BF16)
-        for i in range(low_i, high_i):
+        for i in range(high_i - 1, low_i - 1, -1):
+            for b in peers:
+                sending[i, b] = (mine[i, b] + given[i, b].astype(F32)).astype(BF16)
+        for i in range(high_i - 1, low_i - 1, -1):
             for b in peers:
                 part(i, b).start()
 
     def whole(i):
-        total = mine[i, 0]
+        total = mine[i, 0] + given[i, 0].astype(F32)
         for b in peers:
             part(i, b).wait_recv()
             total += landed[i, b].astype(F32)
@@ -254,12 +254,12 @@
         depart(c - 1)
         ready(c)
         compute(c)
-        for i in range(*chunks[c - 1]):
+        for i in reversed(range(*chunks[c - 1])):
             if i > 0:
                 summed[i] = whole(i).astype(BF16)
                 last(i).start()
     depart(len(chunks) - 1)
-    for i in range(*chunks[-1]):
+    for i in reversed(range(*chunks[-1])):
         if i > 0:
             summed[i] = whole(i).astype(BF16)
             last(i).start()

time: 32.3 us -> 31.8 us (0.985)
  Pallas kernels: 30.6 us -> 30.2 us
    pallas_call x1, Pallas kernels: 30.6 us -> 30.2 us  [per_device(): pl.pallas_call(functools.partial(kernel, n, plane), out_shape=jax.ShapeDt...]
where the time goes in v4:
time: 31.8 us; the launch traced here: 31.6 us
  Pallas kernels  30.2 us (95%)
  local copies, waits for them, and re-layouts  1.38 us (4%)
    pallas_call x1, Pallas kernels, per_device(): pl.pallas_call(functools.partial(kernel, n, plane), out_shape=jax.ShapeDt...  30.2 us
    unnamed x1, local copies, waits for them, and re-layouts  1.38 us

profile of v4, /device:TPU:0, one launch (start us, length us, event | category | flops | bytes accessed | tf_op | source)
XLA Modules:
  0.0 31.6 jit_solution(12577869367118625021)
XLA Ops:
  0.0 30.2 %shard_map.109 = bf16[8,2048]{1,0:T(8,128)(2,1)} custom-call(bf16[8,2048]{1,0:T(8,128)(2,1)} %tokens.1, f32[1,2048]{1,0:T(1,128)} %bitcast.5, bf16[2048]{0:T(1024)(128)(2,1)} %branch.1, s32[8,8]{1,0:T(8,128)} %route.1, f32[8,8]{1,0:T(8,128)} %weight.1, bf16[1,2048,640]{2,1,0:T(8,128)(2,1)} %e_gate.1, bf16[1,2048,640]{2,1,0:T(8,128)(2,1)} %e_up.1, ...), custom_call_target="tpu_custom_call" | custom-call | tf_op jit(solution)/shard_map/pallas_call | solution.py:312
  30.2 1.4 %copy.13 = bf16[8,2048]{1,0:T(8,128)(2,1)} copy(bf16[8,2048]{1,0:T(8,128)(2,1)} %shard_map.109) | data formatting | bytes 65536
